TPU v7x, 32 devices: a whole 2x2x4 slice. The times are simulated.
32 devices in a mesh: grp: 2 (over y), sp: 4 (over z), tp: 4 (over x, core).
Axes of the slice: x: 2, y: 2, z: 4, core: 2. Of those that a mesh axis runs over, the one named last changes fastest.
Arguments:
- tokens: bfloat16 [4096, 2048], P(('grp', 'sp')), parts along dimension 0, may hold values from -6 to 6
- fresh_token_input: bfloat16 [4096], P('grp'), parts along dimension 0, may hold values from -6 to 6
- value_matrix: bfloat16 [2048, 2048], P(None, 'tp'), may hold values from -0.125 to 0.125
- write_matrix: bfloat16 [2048, 1024], P(None, 'tp'), may hold values from -0.125 to 0.125
- read_matrix: bfloat16 [2048, 1024], P(None, 'tp'), may hold values from -0.125 to 0.125
- gate_matrix: bfloat16 [2048, 2048], P(None, 'tp'), may hold values from -0.125 to 0.125
- step_matrix: bfloat16 [2048, 32], replicated, may hold values from -0.125 to 0.125
- value_filter_taps: bfloat16 [4, 2048], replicated, may hold values from -3 to 3
- write_filter_taps: bfloat16 [4, 1024], replicated, may hold values from -3 to 3
- read_filter_taps: bfloat16 [4, 1024], replicated, may hold values from -3 to 3
- head_log_decay: float32 [32], replicated
- step_offset_bias: float32 [32], replicated, may hold values from -3.5 to -2.5
- decay_spike: float32 [4096, 32], P(('grp', 'sp'), 'tp'), parts along dimension 0, may hold values from -3 to 0, as said below
- bypass_scale: float32 [32], replicated, may hold values from 0.5 to 2
- group_norm_scale: float32 [2048], replicated, may hold values from 0.1 to 1.9
Outputs:
- prompt_out: bfloat16 [4096, 2048], P(('grp', 'sp'), 'tp'), parts along dimension 0
- state_cache: bfloat16 [256, 2048], P(('grp', 'sp'), 'tp'), parts along dimension 0
- step_out: bfloat16 [1024, 4], P(('grp', 'tp'), 'sp'), parts along dimension 0
There are 2 independent parts, one for each index of `grp`. A program takes and returns all parts, laid end to end along the dimension named above; an argument that names none is the same for every part. Nothing has to cross between parts.
Inputs may be any that keep to these rules, and one draw needn't show every extreme that they name: `decay_spike`: never positive.
All inputs are finite; a program needn't handle non-finite values.
Results may differ from a plain program's by a relative error of at most 0.023.
Values may be sent and summed in bfloat16 or wider, within the bound.
A program may use at most 64 MiB of HBM per device.

v0:
```python
import jax
import jax.numpy as jnp
from jax import lax
from jax.sharding import PartitionSpec as P

HEAD = 64
STATE = 128
CONV = 4
BLOCK = 128
epsilon = 1e-06


def passed_along(block, axis, distance):
    devices = range(lax.axis_size(axis))
    route = [(i - distance, i) for i in devices if i - distance in devices]
    return lax.ppermute(block, axis, route)


def from_root(value, axis, source):
    kept = jnp.where(lax.axis_index(axis) == source, value, 0).astype(value.dtype)
    return lax.psum(kept, axis)


def project(operand, weights):
    return jnp.dot(operand, weights, preferred_element_type=jnp.float32).astype(jnp.bfloat16)


def apply_taps(previous, current, tap_weights):
    joined = jnp.concatenate([previous, current], axis=0).astype(jnp.float32)
    length = current.shape[0]
    summed = jnp.zeros(current.shape, jnp.float32)
    for offset in range(CONV):
        summed = summed + tap_weights[offset].astype(jnp.float32) * joined[offset : offset + length]
    return summed


def group_norm(gated_rows, groups):
    shaped = gated_rows.reshape(gated_rows.shape[:-1] + (groups, -1))
    normed = shaped * lax.rsqrt(jnp.mean(shaped * shaped, axis=-1, keepdims=True) + epsilon)
    return normed.reshape(gated_rows.shape)


def read_new(cached, stored_portion, read_part, new_decay, step_now, value_now):
    states = cached.astype(jnp.float32).reshape((cached.shape[0],) + value_now.shape)
    updated = (
        new_decay[None, :, :, None] * states
        + step_now[None, :, :, None] * stored_portion.T[:, :, None, None] * value_now[None]
    )
    return jnp.einsum("gn,ngep->gep", read_part, updated, precision=lax.Precision.HIGHEST)


def on_device(
    tokens,
    fresh_token_input,
    value_matrix,
    write_matrix,
    read_matrix,
    gate_matrix,
    step_matrix,
    value_filter_taps,
    write_filter_taps,
    read_filter_taps,
    head_log_decay,
    step_offset_bias,
    decay_spike,
    bypass_scale,
    group_norm_scale,
):
    head_rank = lax.axis_index("tp")
    sequence_rank = lax.axis_index("sp")
    sequence_count = lax.axis_size("sp")
    channels = value_matrix.shape[1]
    head_count = channels // HEAD
    map_width = write_matrix.shape[1]
    group_count = map_width // STATE
    per_group = head_count // group_count
    row_count = tokens.shape[0]
    head_start = head_rank * head_count
    local_count = STATE // sequence_count
    own_step = lax.dynamic_slice_in_dim(step_matrix, head_start, head_count, 1)
    own_value_taps = lax.dynamic_slice_in_dim(value_filter_taps, head_rank * channels, channels, 1)
    own_write_taps = lax.dynamic_slice_in_dim(
        write_filter_taps, head_rank * map_width, map_width, 1
    )
    own_read_taps = lax.dynamic_slice_in_dim(read_filter_taps, head_rank * map_width, map_width, 1)
    head_decay_rates = jnp.exp(lax.dynamic_slice_in_dim(head_log_decay, head_start, head_count, 0))
    own_bias = lax.dynamic_slice_in_dim(step_offset_bias, head_start, head_count, 0)
    own_skip = lax.dynamic_slice_in_dim(bypass_scale, head_start, head_count, 0)
    own_gain = lax.dynamic_slice_in_dim(group_norm_scale, head_rank * channels, channels, 0)
    value_rows = project(tokens, value_matrix)
    write_rows = project(tokens, write_matrix)
    read_rows = project(tokens, read_matrix)
    gate_rows = project(tokens, gate_matrix)
    step_raw = jnp.dot(tokens, own_step, preferred_element_type=jnp.float32)
    edge = row_count - (CONV - 1)
    tail_rows = (value_rows[edge:], write_rows[edge:], read_rows[edge:])
    before = passed_along((tail_rows[0], tail_rows[1], tail_rows[2]), "sp", 1)
    ending = (
        from_root(tail_rows[0], "sp", sequence_count - 1),
        from_root(tail_rows[1], "sp", sequence_count - 1),
        from_root(tail_rows[2], "sp", sequence_count - 1),
    )
    values = jax.nn.silu(apply_taps(before[0], value_rows, own_value_taps)).astype(jnp.bfloat16)
    writes = jax.nn.silu(apply_taps(before[1], write_rows, own_write_taps)).astype(jnp.bfloat16)
    reads = jax.nn.silu(apply_taps(before[2], read_rows, own_read_taps)).astype(jnp.bfloat16)
    step_length = jax.nn.softplus(step_raw + own_bias)
    log_decay_value = decay_spike - step_length * head_decay_rates
    blocks = row_count // BLOCK
    block_values = values.reshape(blocks, BLOCK, group_count, per_group, HEAD)
    block_writes = writes.reshape(blocks, BLOCK, group_count, STATE)
    block_reads = reads.reshape(blocks, BLOCK, group_count, STATE)
    block_steps = step_length.reshape(blocks, BLOCK, group_count, per_group)
    cumulative = jnp.cumsum(log_decay_value.reshape(blocks, BLOCK, group_count, per_group), axis=1)
    block_end = cumulative[:, -1]
    scaled = (
        (jnp.exp(block_end[:, None] - cumulative) * block_steps)[..., None]
        * block_values.astype(jnp.float32)
    ).astype(jnp.bfloat16)
    block_states = jnp.einsum(
        "bsgn,bsgep->bngep", block_writes, scaled, preferred_element_type=jnp.float32
    )
    running = jnp.zeros((STATE, group_count, per_group, HEAD), jnp.float32)
    inside = []
    for block_index in range(blocks):
        inside.append(running)
        running = (
            jnp.exp(block_end[block_index])[None, :, :, None] * running + block_states[block_index]
        )
    local_states = jnp.stack(inside)
    shard_fading_factor = jnp.sum(block_end, axis=0)
    before_block = jnp.cumsum(block_end, axis=0) - block_end
    decay_table = lax.all_gather(shard_fading_factor[None], "sp", axis=0, tiled=True)
    inclusive = jnp.cumsum(decay_table, axis=0)
    exclusive = inclusive - decay_table
    total_decay = inclusive[-1]
    row_pieces = lax.all_to_all(running[None], "sp", split_axis=1, concat_axis=0, tiled=True)
    ranks = jnp.arange(sequence_count)
    below = (ranks[None, :] < ranks[:, None])[:, :, None, None]
    prefix_weight = jnp.exp(jnp.where(below, exclusive[:, None] - inclusive[None, :], -jnp.inf))
    prefix_rows = jnp.einsum(
        "jkge,kngep->jngep", prefix_weight, row_pieces, precision=lax.Precision.HIGHEST
    )
    final_weight = jnp.exp(total_decay[None] - inclusive)
    final_rows = jnp.einsum(
        "kge,kngep->ngep", final_weight, row_pieces, precision=lax.Precision.HIGHEST
    )
    earlier_state = lax.all_to_all(prefix_rows, "sp", split_axis=0, concat_axis=1, tiled=True)[0]
    scores = jnp.einsum(
        "blgn,bsgn->bgls", block_reads, block_writes, preferred_element_type=jnp.float32
    )
    cum_heads = jnp.transpose(cumulative, (0, 2, 3, 1))
    decay_gaps = cum_heads[..., :, None] - cum_heads[..., None, :]
    step_heads = jnp.transpose(block_steps, (0, 2, 3, 1))
    causal = jnp.tril(jnp.ones((BLOCK, BLOCK), bool))
    mixing = (
        scores[:, :, None]
        * jnp.exp(jnp.where(causal, decay_gaps, -jnp.inf))
        * step_heads[..., None, :]
    ).astype(jnp.bfloat16)
    inner_part = jnp.einsum(
        "bgels,bsgep->blgep", mixing, block_values, preferred_element_type=jnp.float32
    )
    entering = jnp.exp(before_block)[:, None, :, :, None] * earlier_state[None] + local_states
    carried_part = jnp.exp(cumulative)[..., None] * jnp.einsum(
        "blgn,bngep->blgep",
        block_reads.astype(jnp.float32),
        entering,
        precision=lax.Precision.HIGHEST,
    )
    mixed_rows = (inner_part + carried_part).reshape(row_count, head_count, HEAD) + own_skip[
        None, :, None
    ] * values.astype(jnp.float32).reshape(row_count, head_count, HEAD)
    gated_rows = mixed_rows.reshape(row_count, channels) * jax.nn.silu(
        gate_rows.astype(jnp.float32)
    )
    prompt_out = (group_norm(gated_rows, group_count) * own_gain).astype(jnp.bfloat16)
    new_row = fresh_token_input[None]
    new_value = project(new_row, value_matrix)
    new_write = project(new_row, write_matrix)
    new_read = project(new_row, read_matrix)
    new_gate = project(new_row, gate_matrix)
    new_step = jax.nn.softplus(
        jnp.dot(new_row, own_step, preferred_element_type=jnp.float32)[0] + own_bias
    )
    new_values = jax.nn.silu(apply_taps(ending[0], new_value, own_value_taps)).astype(jnp.bfloat16)
    latest_stores = jax.nn.silu(apply_taps(ending[1], new_write, own_write_taps)).astype(
        jnp.bfloat16
    )
    new_reads = jax.nn.silu(apply_taps(ending[2], new_read, own_read_taps)).astype(jnp.bfloat16)
    value_now = new_values.astype(jnp.float32).reshape(group_count, per_group, HEAD)
    write_now = latest_stores.astype(jnp.float32).reshape(group_count, STATE)
    read_now = new_reads.astype(jnp.float32).reshape(group_count, STATE)
    new_decay = jnp.exp(-new_step * head_decay_rates).reshape(group_count, per_group)
    step_now = new_step.reshape(group_count, per_group)
    row_start = sequence_rank * local_count
    cache_rows = final_rows.reshape(local_count, channels).astype(jnp.bfloat16)
    stored_portion = lax.dynamic_slice_in_dim(write_now, row_start, local_count, 1)
    read_part = lax.dynamic_slice_in_dim(read_now, row_start, local_count, 1)
    partial_value = read_new(cache_rows, stored_portion, read_part, new_decay, step_now, value_now)
    reading = lax.psum(partial_value, "sp")
    new_mixed = reading + own_skip.reshape(group_count, per_group)[:, :, None] * value_now
    new_gated = new_mixed.reshape(1, channels) * jax.nn.silu(new_gate.astype(jnp.float32))
    step_whole = (group_norm(new_gated, group_count) * own_gain).astype(jnp.bfloat16)[0]
    step_table = step_whole.reshape(channels // sequence_count, sequence_count)
    step_out = lax.dynamic_slice_in_dim(step_table, sequence_rank, 1, 1)
    return (prompt_out, cache_rows, step_out)


def solution(mesh):
    placed = (
        P(("grp", "sp"), None),
        P("grp"),
        P(None, "tp"),
        P(None, "tp"),
        P(None, "tp"),
        P(None, "tp"),
        P(),
        P(),
        P(),
        P(),
        P(),
        P(),
        P(("grp", "sp"), "tp"),
        P(),
        P(),
    )
    return jax.shard_map(
        on_device,
        mesh=mesh,
        in_specs=placed,
        out_specs=(P(("grp", "sp"), "tp"), P(("grp", "sp"), "tp"), P(("grp", "tp"), "sp")),
        check_vma=False,
    )
```

profile of v0, /device:TPU:0, one launch (start us, length us, event | category | flops | bytes accessed | tf_op | source)
XLA Modules:
  0.0 126.4 jit_solution(4960432107386798171)
XLA Ops:
  0.7 1.6 %copy-done = bf16[512,2048]{1,0:T(8,128)(2,1)S(1)} copy-done((bf16[512,2048]{1,0:T(8,128)(2,1)S(1)}, bf16[512,2048]{1,0:T(8,128)(2,1)}, u32[]{:S(2)}) %copy-start) | copy-done | bytes 2097176
  2.2 1.9 %convolution_convert_fusion.2 = bf16[512,256]{1,0:T(8,128)(2,1)S(1)} fusion(bf16[512,2048]{1,0:T(8,128)(2,1)S(1)} %copy-done, bf16[2048,256]{1,0:T(8,128)(2,1)} %param.18), kind=kOutput, calls=%fused_computation.11 | convolution fusion | flops 537001984 | bytes 3407872 | tf_op jit(solution)/shard_map/dot_general | solution.py:25
  4.2 0.6 broadcast_select_fusion.1
  4.7 5.7 %collective-permute-start.2 = (bf16[3,256]{1,0:T(4,128)(2,1)}, bf16[3,256]{1,0:T(4,128)(2,1)}, u32[]{:S(2)}, u32[]{:S(2)}) collective-permute-start(bf16[3,256]{1,0:T(4,128)(2,1)} %get-tuple-element.57), channel_id=1, source_target_pairs={{0,4},{4,8},{8,12},{1,5},{5,9},{9,13},{2,6},{6,10},{10,14},{3,7},{... | collective-permute-start | bytes 4616 | tf_op jit(solution)/shard_map/ppermute | solution.py:16
  10.4 0.7 convolution_convert_fusion.3
  11.1 0.6 fusion.92
  11.8 3.6 %collective-permute-start.1 = (bf16[3,256]{1,0:T(4,128)(2,1)}, bf16[3,256]{1,0:T(4,128)(2,1)}, u32[]{:S(2)}, u32[]{:S(2)}) collective-permute-start(bf16[3,256]{1,0:T(4,128)(2,1)} %get-tuple-element.54), channel_id=1, source_target_pairs={{0,4},{4,8},{8,12},{1,5},{5,9},{9,13},{2,6},{6,10},{10,14},{3,7},{... | collective-permute-start | bytes 4616 | tf_op jit(solution)/shard_map/ppermute | solution.py:16
  15.4 1.3 convolution_convert_fusion.1
  16.7 0.8 copy-done.8
  17.5 0.6 fusion.91
  18.1 3.5 %collective-permute-start = (bf16[3,512]{1,0:T(4,128)(2,1)}, bf16[3,512]{1,0:T(4,128)(2,1)}, u32[]{:S(2)}, u32[]{:S(2)}) collective-permute-start(bf16[3,512]{1,0:T(4,128)(2,1)} %get-tuple-element.52), channel_id=1, source_target_pairs={{0,4},{4,8},{8,12},{1,5},{5,9},{9,13},{2,6},{6,10},{10,14},{3,7},{... | collective-permute-start | bytes 9224 | tf_op jit(solution)/shard_map/ppermute | solution.py:16
  21.6 0.5 iota_compare_fusion.1
  22.4 1.5 %fusion.96 = f32[1,256]{1,0:T(1,128)S(1)} fusion(bf16[2048,1]{0,1:T(2,128)(2,1)S(1)} %reshape.251, bf16[2048,256]{1,0:T(8,128)(2,1)} %param.19), kind=kOutput, calls=%fused_computation.194 | convolution fusion | flops 1048576 | bytes 1053696 | tf_op jit(solution)/shard_map/dot_general | solution.py:25
  24.5 0.7 multiply_exponential_fusion
  25.1 0.7 multiply_subtract_fusion
  26.3 0.6 fusion.76
  27.1 2.0 %fusion.99 = f32[1,512]{1,0:T(1,128)S(1)} fusion(bf16[2048,1]{0,1:T(2,128)(2,1)S(1)} %reshape.251, bf16[2048,512]{1,0:T(8,128)(2,1)} %param.20), kind=kOutput, calls=%fused_computation.197 | convolution fusion | flops 2097152 | bytes 2103296 | tf_op jit(solution)/shard_map/dot_general | solution.py:25
  29.1 7.6 %all-gather.1 = f32[4,2,4]{2,1,0:T(2,128)S(1)} all-gather(f32[1,2,4]{2,1,0:T(2,128)S(1)} %bitcast.152), channel_id=2, replica_groups=mesh['grp'=2,'sp'=4,'tp'=4] {'sp'}, dimensions={0}, use_global_device_ids=true | all-gather | bytes 160 | tf_op jit(solution)/shard_map/all_gather | solution.py:132
  36.7 10.5 %all-reduce = (bf16[3,512]{1,0:T(4,128)(2,1)S(1)}, bf16[3,256]{1,0:T(4,128)(2,1)S(1)}, bf16[3,256]{1,0:T(4,128)(2,1)S(1)}) all-reduce(bf16[3,512]{1,0:T(4,128)(2,1)S(1)} %get-tuple-element.53, bf16[3,256]{1,0:T(4,128)(2,1)S(1)} %get-tuple-element.56, ...), channel_id=1, replica_groups=mesh['grp'=2,'sp'=4,'tp'=4] {'sp'}, use_global_device_ids=true, to_apply=%region_7.8 | all-reduce | flops 3072 | bytes 12288 | tf_op jit(solution)/shard_map/psum | solution.py:21
  47.3 0.7 convert_convert_fusion
  48.1 1.0 copy.149
  49.2 0.7 convert_reduce_fusion.1
  49.9 2.4 %fusion.90 = (f32[4,128,2,4]{3,2,1,0:T(2,128)}, f32[4,128,2,4]{3,2,1,0:T(2,128)S(1)}) fusion(f32[4,128,2,4]{3,2,1,0:T(2,128)S(1)} %fusion.94, f32[4,128,2,4]{3,2,1,0:T(2,128)} %copy.149, f32[4,2,4]{2,1,0:T(2,128)S(1)} %get-tuple-element.47), kind=kLoop, calls=%fused_computation.187 | loop fusion | flops 8192 | bytes 65664 | tf_op jit(solution)/shard_map/exp | solution.py:164
  52.4 0.7 convert_reduce_fusion
  53.0 0.6 fusion.81
  53.7 0.7 dynamic_slice.39
  54.5 0.7 mul.552
  55.2 0.7 mul.510
  55.9 1.3 %mul.529 = f32[2,4]{1,0:T(2,128)} reshape(f32[8]{0:T(128)} %get-tuple-element.28) | data formatting | bytes 64 | tf_op jit(solution)/shard_map/mul | solution.py:46
  57.6 1.3 %copy.148 = f32[4,128,2,4]{1,3,2,0:T(4,128)S(1)} copy(f32[4,128,2,4]{3,2,1,0:T(2,128)} %get-tuple-element.44) | data formatting | bytes 32768 | tf_op jit(solution)/shard_map/exp | solution.py:164
  59.1 0.6 pad.6.clone
  59.7 0.7 maximum_convert_fusion.2
  60.5 1.0 multiply_convert_fusion.5
  61.5 0.8 maximum_convert_fusion.1
  62.8 0.8 maximum_convert_fusion
  63.6 1.3 %multiply_convert_fusion.4 = bf16[512,512]{1,0:T(8,128)(2,1)S(1)} fusion(f32[515,512]{1,0:T(8,128)S(1)} %maximum_convert_fusion, f32[512]{0:T(512)} %bitcast.141, f32[512]{0:T(512)} %bitcast.140, f32[512]{0:T(512)S(1)} %bitcast.139, f32[512]{0:T(512)S(1)} %bitcast.138), kind=kLoop, calls=%fused_computation.44 | loop fusion | flops 3145728 | bytes 4726784 | tf_op jit(solution)/shard_map/convert_element_type | solution.py:103
  65.0 1.0 copy.140
  66.0 2.0 %reshape.229 = bf16[4,128,2,4,64]{1,0,4,3,2:T(4,128)(2,1)} reshape(bf16[512,512]{0,1:T(8,128)(2,1)} %copy.140) | data formatting | bytes 1048576 | tf_op jit(solution)/shard_map/reshape | solution.py:109
  68.0 1.3 multiply_convert_fusion.3
  69.5 1.0 slice_add_fusion
  70.8 1.2 reshape.274
  72.0 3.6 %all-to-all-start = ((f32[4,1,16384]{2,1,0:T(1,128)}), f32[4,1,16384]{2,1,0:T(1,128)S(1)}, u32[]{:S(2)}, u32[]{:S(2)}) async-start(f32[4,1,16384]{2,1,0:T(1,128)} %reshape.274), calls=%async_computation | async-start | bytes 524288 | tf_op jit(solution)/shard_map/all_to_all | solution.py:136
  75.9 3.0 %convolution_bitcast_fusion.2 = f32[4,128,2,4,64]{1,4,3,2,0:T(8,128)} fusion(f32[4,2,4,128]{3,2,1,0:T(4,128)S(1)} %copy.146, f32[4,2,4,128]{3,2,1,0:T(4,128)S(1)} %copy.144, f32[4,2,128,128]{3,2,1,0:T(8,128)S(1)} %fusion.40, pred[128,128]{1,0:T(8,128)(4,1)S(1)} %iota_compare_fusion, bf16[4,128,2,4,64]{1,0,4,3,2:T(4,128)(2,1)} %reshape.229), kind=kOutput, calls=%fused_computation.5 | convolution fusion | flops 69730304 | bytes 2146304 | tf_op jit(solution)/shard_map/bgels,bsgep->blgep/dot_general | solution.py:160
  78.8 3.3 %all-to-all-done = f32[4,1,16384]{2,1,0:T(1,128)S(1)} async-done(((f32[4,1,16384]{2,1,0:T(1,128)}), f32[4,1,16384]{2,1,0:T(1,128)S(1)}, u32[]{:S(2)}, u32[]{:S(2)}) %all-to-all-start) | async-done | bytes 262176 | tf_op jit(solution)/shard_map/all_to_all | solution.py:136
  82.1 0.5 broadcast.118
  82.7 1.3 %reduce.9 = f32[4,16384]{1,0:T(4,128)S(1)} reduce(f32[4,1,16384]{2,1,0:T(1,128)S(1)} %all-to-all-done, f32[]{:T(128)} %broadcast.118), dimensions={1}, to_apply=%all_to_all.6.reduce_sub_computation | reduce | bytes 524292 | tf_op jit(solution)/shard_map/all_to_all | solution.py:136
  84.4 1.3 %fusion.35 = bf16[2,4,1,32,64]{4,2,3,1,0:T(2,128)(2,1)S(1)} fusion(f32[4,2,4,1,1]{0,3,4,2,1:T(1,128)S(1)} %copy.173, f32[4,32,2,4,64]{4,3,2,1,0:T(4,128)S(1)} %bitcast.123), kind=kOutput, calls=%fused_computation.69 | convolution fusion | flops 786432 | bytes 295040 | tf_op jit(solution)/shard_map/kge,kngep->ngep/dot_general | solution.py:144
  85.7 1.3 %convolution_bitcast_fusion.3 = f32[4,32,2,4,64]{4,0,1,3,2:T(4,128)S(1)} fusion(f32[4,32,2,4,64]{4,3,2,1,0:T(4,128)S(1)} %bitcast.124, f32[4,2,4]{0,2,1:T(4,128)S(1)} %copy.156, f32[4,2,4]{0,2,1:T(4,128)S(1)} %copy.155, pred[4,4]{1,0:T(4,128)(4,1)S(1)} %copy-done.30), kind=kOutput, calls=%fused_computation.10 | convolution fusion | flops 3145984 | bytes 524560 | tf_op jit(solution)/shard_map/jkge,kngep->jngep/dot_general | solution.py:140
  87.1 1.0 reshape.276
  88.1 3.4 %all-to-all-start.1 = ((f32[4,1,16384]{2,1,0:T(1,128)}), f32[4,1,16384]{2,1,0:T(1,128)S(1)}, u32[]{:S(2)}, u32[]{:S(2)}) async-start(f32[4,1,16384]{2,1,0:T(1,128)} %reshape.276), calls=%async_computation.1 | async-start | bytes 524288 | tf_op jit(solution)/shard_map/all_to_all | solution.py:147
  91.9 12.2 %psum.31 = f32[2,4,64]{2,1,0:T(4,128)S(1)} all-reduce(f32[2,4,64]{2,1,0:T(4,128)S(1)} %bitcast.137), channel_id=1, replica_groups=mesh['grp'=2,'sp'=4,'tp'=4] {'sp'}, use_global_device_ids=true, to_apply=%region_8.9 | all-reduce | flops 512 | bytes 4096 | tf_op jit(solution)/shard_map/psum | solution.py:200
  104.5 0.7 convert_element_type.211
  105.3 0.8 multiply_convert_fusion.7
  106.3 0.6 copy.168
  106.9 1.3 %reduce.10 = f32[4,16384]{1,0:T(4,128)S(1)} reduce(f32[4,1,16384]{2,1,0:T(1,128)S(1)} %all-to-all-done.1, f32[]{:T(128)} %broadcast.118), dimensions={1}, to_apply=%all_to_all.8.reduce_sub_computation | reduce | bytes 524292 | tf_op jit(solution)/shard_map/all_to_all | solution.py:147
  108.5 0.9 copy.160
  109.4 2.3 %fusion.1 = f32[4,128,2,4,64]{1,4,3,2,0:T(8,128)S(1)} fusion(f32[4,128,2,4,64]{1,4,3,2,0:T(8,128)} %convolution_bitcast_fusion.2, f32[1,128,2,4,64]{1,4,3,2,0:T(8,128)} %get-tuple-element.41, f32[1,128,2,4,64]{1,4,3,2,0:T(8,128)} %get-tuple-element.42, f32[1,128,2,4,64]{1,4,3,2,0:T(8,128)} %get-tuple-element.43, f32[4]{0:T(128)S(1)} %copy-done.31, ...), kind=kOutput, calls=%fused_computation.4 | convolution fusion | flops 404488192 | bytes 3424400 | tf_op jit(solution)/shard_map/blgn,bngep->blgep/dot_general | solution.py:164
  111.7 1.8 %copy.184 = f32[4,128,2,4,64]{4,3,2,1,0:T(4,128)} copy(f32[4,128,2,4,64]{1,4,3,2,0:T(8,128)S(1)} %fusion.1) | data formatting | bytes 2097152 | tf_op jit(solution)/shard_map/reshape | solution.py:170
  113.5 3.5 %reshape.263 = f32[512,512]{1,0:T(8,128)} reshape(f32[4,128,2,4,64]{4,3,2,1,0:T(4,128)} %copy.184) | data formatting | bytes 2097152 | tf_op jit(solution)/shard_map/reshape | solution.py:170
  117.0 4.6 %fusion.93 = (f32[512,512]{1,0:T(8,128)}, f32[512,512]{1,0:T(8,128)}) fusion(bf16[512,2048]{1,0:T(8,128)(2,1)S(1)} %copy-done, bf16[2048,512]{1,0:T(8,128)(2,1)} %param.20, f32[512,512]{1,0:T(8,128)} %reshape.263, bf16[512,512]{1,0:T(8,128)(2,1)S(1)} %copy-done.2, f32[512]{0:T(512)S(1)} %copy-done.25), kind=kOutput, calls=%fused_computation.190 | convolution fusion | flops 1076625408 | bytes 7866368 | tf_op jit(solution)/shard_map/dot_general | solution.py:25
  121.7 1.9 %mul.516 = f32[512,2,256]{2,1,0:T(2,128)S(1)} reshape(f32[512,512]{1,0:T(8,128)} %get-tuple-element.63) | data formatting | bytes 2097152 | tf_op jit(solution)/shard_map/mul | solution.py:39
  123.5 0.6 reduce_sum.28
  124.2 0.6 mul.517
  125.4 1.1 multiply_convert_fusion.2
  (128 shorter events, 6.4 us)
Async XLA Ops:
  0.6 1.6 %copy-start = (bf16[512,2048]{1,0:T(8,128)(2,1)S(1)}, bf16[512,2048]{1,0:T(8,128)(2,1)}, u32[]{:S(2)}) copy-start(bf16[512,2048]{1,0:T(8,128)(2,1)} %param.15) | copy-start | bytes 6291460
  0.6 9.8 %copy-start.6 = (bf16[2048,256]{1,0:T(8,128)(2,1)S(1)}, bf16[2048,256]{1,0:T(8,128)(2,1)}, u32[]{:S(2)}) copy-start(bf16[2048,256]{1,0:T(8,128)(2,1)} %param.19) | copy-start | bytes 3145732
  4.2 11.3 %copy-start.3 = (bf16[2048,512]{1,0:T(8,128)(2,1)S(1)}, bf16[2048,512]{1,0:T(8,128)(2,1)}, u32[]{:S(2)}) copy-start(bf16[2048,512]{1,0:T(8,128)(2,1)} %param.17) | copy-start | bytes 6291460
  4.7 55.0 %collective-permute-start.2 = (bf16[3,256]{1,0:T(4,128)(2,1)}, bf16[3,256]{1,0:T(4,128)(2,1)}, u32[]{:S(2)}, u32[]{:S(2)}) collective-permute-start(bf16[3,256]{1,0:T(4,128)(2,1)} %get-tuple-element.57), channel_id=1, source_target_pairs={{0,4},{4,8},{8,12},{1,5},{5,9},{9,13},{2,6},{6,10},{10,14},{3,7},{... | collective-permute-start | bytes 4616 | tf_op jit(solution)/shard_map/ppermute | solution.py:16
  11.1 0.7 copy-start.10
  11.8 10.3 %copy-start.23 = (bf16[2048]{0:T(1024)(128)(2,1)S(1)}, bf16[2048]{0:T(1024)(128)(2,1)}, u32[]{:S(2)}) copy-start(bf16[2048]{0:T(1024)(128)(2,1)} %param.16) | copy-start | bytes 12292
  11.8 10.3 %copy-start.5 = (bf16[2048,256]{1,0:T(8,128)(2,1)S(1)}, bf16[2048,256]{1,0:T(8,128)(2,1)}, u32[]{:S(2)}) copy-start(bf16[2048,256]{1,0:T(8,128)(2,1)} %param.18) | copy-start | bytes 3145732
  11.8 49.6 %collective-permute-start.1 = (bf16[3,256]{1,0:T(4,128)(2,1)}, bf16[3,256]{1,0:T(4,128)(2,1)}, u32[]{:S(2)}, u32[]{:S(2)}) collective-permute-start(bf16[3,256]{1,0:T(4,128)(2,1)} %get-tuple-element.54), channel_id=1, source_target_pairs={{0,4},{4,8},{8,12},{1,5},{5,9},{9,13},{2,6},{6,10},{10,14},{3,7},{... | collective-permute-start | bytes 4616 | tf_op jit(solution)/shard_map/ppermute | solution.py:16
  16.7 0.8 copy-start.8
  18.1 44.7 %collective-permute-start = (bf16[3,512]{1,0:T(4,128)(2,1)}, bf16[3,512]{1,0:T(4,128)(2,1)}, u32[]{:S(2)}, u32[]{:S(2)}) collective-permute-start(bf16[3,512]{1,0:T(4,128)(2,1)} %get-tuple-element.52), channel_id=1, source_target_pairs={{0,4},{4,8},{8,12},{1,5},{5,9},{9,13},{2,6},{6,10},{10,14},{3,7},{... | collective-permute-start | bytes 9224 | tf_op jit(solution)/shard_map/ppermute | solution.py:16
  21.6 2.3 %copy-start.4 = (bf16[2048,512]{1,0:T(8,128)(2,1)S(1)}, bf16[2048,512]{1,0:T(8,128)(2,1)}, u32[]{:S(2)}) copy-start(bf16[2048,512]{1,0:T(8,128)(2,1)} %param.17) | copy-start | bytes 6291460
  22.1 2.2 %copy-start.33 = (f32[32]{0:T(128)S(1)}, f32[32]{0:T(128)}, u32[]{:S(2)}) copy-start(f32[32]{0:T(128)} %param.26) | copy-start | bytes 388
  22.2 2.3 %copy-start.32 = (f32[32]{0:T(128)S(1)}, f32[32]{0:T(128)}, u32[]{:S(2)}) copy-start(f32[32]{0:T(128)} %param.25) | copy-start | bytes 388
  22.2 3.0 %copy-start.12 = (f32[512,8]{0,1:T(8,128)S(1)}, f32[512,8]{0,1:T(8,128)}, u32[]{:S(2)}) copy-start(f32[512,8]{0,1:T(8,128)} %param.27) | copy-start | bytes 49156
  22.4 2.0 %copy-start.13 = (bf16[2048,32]{0,1:T(8,128)(2,1)S(1)}, bf16[2048,32]{0,1:T(8,128)(2,1)}, u32[]{:S(2)}) copy-start(bf16[2048,32]{0,1:T(8,128)(2,1)} %param.21) | copy-start | bytes 393220
  25.8 21.5 %copy-start.26 = (bf16[4,1024]{1,0:T(4,128)(2,1)S(1)}, bf16[4,1024]{1,0:T(4,128)(2,1)}, u32[]{:S(2)}) copy-start(bf16[4,1024]{1,0:T(4,128)(2,1)} %param.23) | copy-start | bytes 24580
  26.1 23.0 %copy-start.27 = (bf16[4,1024]{1,0:T(4,128)(2,1)S(1)}, bf16[4,1024]{1,0:T(4,128)(2,1)}, u32[]{:S(2)}) copy-start(bf16[4,1024]{1,0:T(4,128)(2,1)} %param.24) | copy-start | bytes 24580
  27.1 25.3 %copy-start.22 = (bf16[4,2048]{1,0:T(4,128)(2,1)S(1)}, bf16[4,2048]{1,0:T(4,128)(2,1)}, u32[]{:S(2)}) copy-start(bf16[4,2048]{1,0:T(4,128)(2,1)} %param.22) | copy-start | bytes 49156
  57.6 3.9 %copy-start.11 = (bf16[512,256]{1,0:T(8,128)(2,1)S(1)}, bf16[512,256]{1,0:T(8,128)(2,1)}, u32[]{:S(2)}) copy-start(bf16[512,256]{1,0:T(8,128)(2,1)} %copy-done.10) | copy-start | bytes 786436
  59.1 3.1 %copy-start.18 = (f32[1,256]{1,0:T(1,128)S(1)}, f32[1,256]{1,0:T(1,128)}, u32[]{:S(2)}) copy-start(f32[1,256]{1,0:T(1,128)} %get-tuple-element.24) | copy-start | bytes 3076
  59.1 3.2 %copy-start.19 = (f32[1,256]{1,0:T(1,128)S(1)}, f32[1,256]{1,0:T(1,128)}, u32[]{:S(2)}) copy-start(f32[1,256]{1,0:T(1,128)} %get-tuple-element.25) | copy-start | bytes 3076
  59.1 3.2 %copy-start.20 = (f32[1,256]{1,0:T(1,128)S(1)}, f32[1,256]{1,0:T(1,128)}, u32[]{:S(2)}) copy-start(f32[1,256]{1,0:T(1,128)} %get-tuple-element.26) | copy-start | bytes 3076
  59.1 3.2 %copy-start.21 = (f32[1,256]{1,0:T(1,128)S(1)}, f32[1,256]{1,0:T(1,128)}, u32[]{:S(2)}) copy-start(f32[1,256]{1,0:T(1,128)} %get-tuple-element.27) | copy-start | bytes 3076
  61.5 1.3 %copy-start.9 = (bf16[512,512]{1,0:T(8,128)(2,1)S(1)}, bf16[512,512]{1,0:T(8,128)(2,1)}, u32[]{:S(2)}) copy-start(bf16[512,512]{1,0:T(8,128)(2,1)} %copy-done.8) | copy-start | bytes 1572868
  65.0 4.5 %copy-start.1 = (bf16[512,512]{1,0:T(8,128)(2,1)}, bf16[512,512]{1,0:T(8,128)(2,1)S(1)}, u32[]{:S(2)}) copy-start(bf16[512,512]{1,0:T(8,128)(2,1)S(1)} %multiply_convert_fusion.4) | copy-start | bytes 1572868
  66.0 3.5 %copy-start.14 = (f32[2,4]{1,0:T(2,128)S(1)}, f32[2,4]{1,0:T(2,128)}, u32[]{:S(2)}) copy-start(f32[2,4]{1,0:T(2,128)} %get-tuple-element.48) | copy-start | bytes 100
  66.0 3.5 %copy-start.15 = (f32[2,4]{1,0:T(2,128)S(1)}, f32[2,4]{1,0:T(2,128)}, u32[]{:S(2)}) copy-start(f32[2,4]{1,0:T(2,128)} %get-tuple-element.49) | copy-start | bytes 100
  68.0 1.6 %copy-start.16 = (f32[2,4]{1,0:T(2,128)S(1)}, f32[2,4]{1,0:T(2,128)}, u32[]{:S(2)}) copy-start(f32[2,4]{1,0:T(2,128)} %get-tuple-element.50) | copy-start | bytes 100
  68.0 1.6 %copy-start.17 = (f32[2,4]{1,0:T(2,128)S(1)}, f32[2,4]{1,0:T(2,128)}, u32[]{:S(2)}) copy-start(f32[2,4]{1,0:T(2,128)} %get-tuple-element.51) | copy-start | bytes 100
  72.0 10.2 %all-to-all-start = ((f32[4,1,16384]{2,1,0:T(1,128)}), f32[4,1,16384]{2,1,0:T(1,128)S(1)}, u32[]{:S(2)}, u32[]{:S(2)}) async-start(f32[4,1,16384]{2,1,0:T(1,128)} %reshape.274), calls=%async_computation | async-start | bytes 524288 | tf_op jit(solution)/shard_map/all_to_all | solution.py:136
  75.9 9.8 %copy-start.30 = (pred[4,4]{1,0:T(4,128)(4,1)S(1)}, pred[4,4]{1,0:T(4,128)(4,1)}, u32[]{:S(2)}) copy-start(pred[4,4]{1,0:T(4,128)(4,1)} %iota_compare_fusion.1) | copy-start | bytes 52
  84.3 7.2 %copy-start.28 = (f32[2,4]{1,0:T(2,128)S(1)}, f32[2,4]{1,0:T(2,128)}, u32[]{:S(2)}) copy-start(f32[2,4]{1,0:T(2,128)} %mul.529) | copy-start | bytes 100
  84.3 7.4 %copy-start.24 = (bf16[2,32,1,1]{1,0,2,3:T(2,128)(2,1)S(1)}, bf16[2,32,1,1]{1,0,2,3:T(2,128)(2,1)}, u32[]{:S(2)}) copy-start(bf16[2,32,1,1]{1,0,2,3:T(2,128)(2,1)} %fusion.81) | copy-start | bytes 388
  85.7 18.4 %copy-start.29 = (f32[2,4]{1,0:T(2,128)S(1)}, f32[2,4]{1,0:T(2,128)}, u32[]{:S(2)}) copy-start(f32[2,4]{1,0:T(2,128)} %mul.552) | copy-start | bytes 100
  88.1 18.8 %all-to-all-start.1 = ((f32[4,1,16384]{2,1,0:T(1,128)}), f32[4,1,16384]{2,1,0:T(1,128)S(1)}, u32[]{:S(2)}, u32[]{:S(2)}) async-start(f32[4,1,16384]{2,1,0:T(1,128)} %reshape.276), calls=%async_computation.1 | async-start | bytes 524288 | tf_op jit(solution)/shard_map/all_to_all | solution.py:147
  91.5 17.9 %copy-start.31 = (f32[4]{0:T(128)S(1)}, f32[4]{0:T(128)}, u32[]{:S(2)}) copy-start(f32[4]{0:T(128)} %pad.6.clone) | copy-start | bytes 52
  113.5 3.5 %copy-start.2 = (bf16[512,512]{1,0:T(8,128)(2,1)S(1)}, bf16[512,512]{1,0:T(8,128)(2,1)}, u32[]{:S(2)}) copy-start(bf16[512,512]{1,0:T(8,128)(2,1)} %copy-done.1) | copy-start | bytes 1572868
  113.5 3.5 %copy-start.25 = (f32[512]{0:T(512)S(1)}, f32[512]{0:T(512)}, u32[]{:S(2)}) copy-start(f32[512]{0:T(512)} %mul.510) | copy-start | bytes 6148
  124.2 1.2 copy-start.7
where the time goes:
time: 127 us; the launch traced here: 126 us
  blocking collectives  30.3 us (24%)
  local copies, waits for them, and re-layouts  28.8 us (23%)
  matrix products  22.6 us (18%)
  other arithmetic  20.4 us (16%)
  starting transfers between devices  19.8 us (16%)
  waiting for transfers between devices  3.3 us (3%)
    ppermute x3, starting transfers between devices, passed_along(): return lax.ppermute(block, axis, route)  12.8 us
    dot_general x8, matrix products, project(): jnp.dot(operand, weights, preferred_element_type=jnp.float32)  12.6 us
    psum x1, blocking collectives, on_device(): reading = lax.psum(partial_value, 'sp')  12.2 us
    psum x1, blocking collectives, from_root(): return lax.psum(kept, axis)  10.5 us
    all_gather x1, blocking collectives, on_device(): lax.all_gather(shard_fading_factor[None], 'sp', axis=0, tiled=True)  7.58 us
    unnamed x75, local copies, waits for them, and re-layouts  6.63 us
    reshape x2, local copies, waits for them, and re-layouts, on_device(): (inner_part + carried_part).reshape(row_count, head_count, HEAD)  5.28 us
    all_to_all x1, starting transfers between devices, on_device(): lax.all_to_all(running[None], 'sp', split_axis=1, concat_axis=0, tiled=True)  3.58 us
  transfers between devices with their start and end apart: 5, of which 1 were waited for; matrix products, arithmetic and copies ran while one was open for 26% of the time, Pallas kernels for 0%

commit v1 on v0

--- a/solution.py
+++ b/solution.py
@@ -197,7 +197,9 @@
     stored_portion = lax.dynamic_slice_in_dim(write_now, row_start, local_count, 1)
     read_part = lax.dynamic_slice_in_dim(read_now, row_start, local_count, 1)
     partial_value = read_new(cache_rows, stored_portion, read_part, new_decay, step_now, value_now)
-    reading = lax.psum(partial_value, "sp")
+    reading = partial_value
+    for hop in (1, 2):
+        reading = reading + lax.ppermute(reading, "sp", [(dev, dev ^ hop) for dev in range(4)])
     new_mixed = reading + own_skip.reshape(group_count, per_group)[:, :, None] * value_now
     new_gated = new_mixed.reshape(1, channels) * jax.nn.silu(new_gate.astype(jnp.float32))
     step_whole = (group_norm(new_gated, group_count) * own_gain).astype(jnp.bfloat16)[0]

time: 127 us -> 126 us (level)
  blocking collectives: 30.3 us -> 18.1 us
  waiting for transfers between devices: 3.3 us -> 7.27 us
  starting transfers between devices: 19.8 us -> 23.6 us
  other arithmetic: 20.4 us -> 22.8 us
    psum x1 -> x0, blocking collectives: 12.2 us -> none  [on_device(): reading = lax.psum(partial_value, 'sp')]
    all_to_all x1, waiting for transfers between devices: 0.01 us -> 3.8 us  [on_device(): lax.all_to_all(prefix_rows, 'sp', split_axis=0, concat_axis=1, tiled=True)]
    ppermute x0 -> x2, starting transfers between devices: none -> 2.86 us  [on_device(): lax.ppermute(reading, 'sp', [(dev, dev ^ hop) for dev in range(4)])]
    unnamed x75 -> x73, local copies, waits for them, and re-layouts: 6.63 us -> 6.56 us
  transfers between devices with their start and end apart: 5 -> 7, of which waited for: 1 -> 2; matrix products, arithmetic and copies ran while one was open for 26% -> 28% of each run, Pallas kernels for 0% -> 0%
where the time goes in v1:
time: 126 us; the launch traced here: 125 us
  local copies, waits for them, and re-layouts  29.2 us (23%)
  starting transfers between devices  23.6 us (19%)
  matrix products  23.1 us (18%)
  other arithmetic  22.8 us (18%)
  blocking collectives  18.1 us (14%)
  waiting for transfers between devices  7.27 us (6%)
    ppermute x3, starting transfers between devices, passed_along(): return lax.ppermute(block, axis, route)  12.8 us
    dot_general x8, matrix products, project(): jnp.dot(operand, weights, preferred_element_type=jnp.float32)  12.6 us
    psum x1, blocking collectives, from_root(): return lax.psum(kept, axis)  10.5 us
    all_gather x1, blocking collectives, on_device(): lax.all_gather(shard_fading_factor[None], 'sp', axis=0, tiled=True)  7.58 us
    unnamed x73, local copies, waits for them, and re-layouts  6.56 us
    reshape x2, local copies, waits for them, and re-layouts, on_device(): (inner_part + carried_part).reshape(row_count, head_count, HEAD)  5.27 us
    all_to_all x1, starting transfers between devices, on_device(): lax.all_to_all(running[None], 'sp', split_axis=1, concat_axis=0, tiled=True)  4.24 us
    all_to_all x1, waiting for transfers between devices, on_device(): lax.all_to_all(prefix_rows, 'sp', split_axis=0, concat_axis=1, tiled=True)  3.8 us
  transfers between devices with their start and end apart: 7, of which 2 were waited for; matrix products, arithmetic and copies ran while one was open for 28% of the time, Pallas kernels for 0%

profile of v1, /device:TPU:0, one launch (start us, length us, event | category | flops | bytes accessed | tf_op | source)
XLA Modules:
  0.0 125.4 jit_solution(8295340781273835069)
XLA Ops:
  0.7 1.6 %copy-done = bf16[512,2048]{1,0:T(8,128)(2,1)S(1)} copy-done((bf16[512,2048]{1,0:T(8,128)(2,1)S(1)}, bf16[512,2048]{1,0:T(8,128)(2,1)}, u32[]{:S(2)}) %copy-start) | copy-done | bytes 2097176
  2.2 1.9 %convolution_convert_fusion.2 = bf16[512,256]{1,0:T(8,128)(2,1)S(1)} fusion(bf16[512,2048]{1,0:T(8,128)(2,1)S(1)} %copy-done, bf16[2048,256]{1,0:T(8,128)(2,1)} %param.18), kind=kOutput, calls=%fused_computation.11 | convolution fusion | flops 537001984 | bytes 3407872 | tf_op jit(solution)/shard_map/dot_general | solution.py:25
  4.2 0.6 broadcast_select_fusion.1
  4.8 5.7 %collective-permute-start.2 = (bf16[3,256]{1,0:T(4,128)(2,1)}, bf16[3,256]{1,0:T(4,128)(2,1)}, u32[]{:S(2)}, u32[]{:S(2)}) collective-permute-start(bf16[3,256]{1,0:T(4,128)(2,1)} %get-tuple-element.57), channel_id=1, source_target_pairs={{0,4},{4,8},{8,12},{1,5},{5,9},{9,13},{2,6},{6,10},{10,14},{3,7},{... | collective-permute-start | bytes 4616 | tf_op jit(solution)/shard_map/ppermute | solution.py:16
  10.5 0.7 convolution_convert_fusion.3
  11.2 0.6 fusion.92
  11.8 3.6 %collective-permute-start.1 = (bf16[3,256]{1,0:T(4,128)(2,1)}, bf16[3,256]{1,0:T(4,128)(2,1)}, u32[]{:S(2)}, u32[]{:S(2)}) collective-permute-start(bf16[3,256]{1,0:T(4,128)(2,1)} %get-tuple-element.54), channel_id=1, source_target_pairs={{0,4},{4,8},{8,12},{1,5},{5,9},{9,13},{2,6},{6,10},{10,14},{3,7},{... | collective-permute-start | bytes 4616 | tf_op jit(solution)/shard_map/ppermute | solution.py:16
  15.4 1.3 %convolution_convert_fusion.1 = bf16[512,512]{1,0:T(8,128)(2,1)S(1)} fusion(bf16[512,2048]{1,0:T(8,128)(2,1)S(1)} %copy-done, bf16[2048,512]{1,0:T(8,128)(2,1)S(1)} %copy-done.3), kind=kOutput, calls=%fused_computation.9 | convolution fusion | flops 1074003968 | bytes 4718592 | tf_op jit(solution)/shard_map/dot_general | solution.py:25
  16.7 0.8 copy-done.8
  17.5 0.6 fusion.91
  18.1 3.5 %collective-permute-start = (bf16[3,512]{1,0:T(4,128)(2,1)}, bf16[3,512]{1,0:T(4,128)(2,1)}, u32[]{:S(2)}, u32[]{:S(2)}) collective-permute-start(bf16[3,512]{1,0:T(4,128)(2,1)} %get-tuple-element.52), channel_id=1, source_target_pairs={{0,4},{4,8},{8,12},{1,5},{5,9},{9,13},{2,6},{6,10},{10,14},{3,7},{... | collective-permute-start | bytes 9224 | tf_op jit(solution)/shard_map/ppermute | solution.py:16
  22.4 1.5 %fusion.96 = f32[1,256]{1,0:T(1,128)S(1)} fusion(bf16[2048,1]{0,1:T(2,128)(2,1)S(1)} %reshape.251, bf16[2048,256]{1,0:T(8,128)(2,1)} %param.19), kind=kOutput, calls=%fused_computation.194 | convolution fusion | flops 1048576 | bytes 1053696 | tf_op jit(solution)/shard_map/dot_general | solution.py:25
  24.6 0.7 multiply_subtract_fusion
  25.8 0.6 fusion.76
  26.5 2.0 %fusion.99 = f32[1,512]{1,0:T(1,128)S(1)} fusion(bf16[2048,1]{0,1:T(2,128)(2,1)S(1)} %reshape.251, bf16[2048,512]{1,0:T(8,128)(2,1)} %param.20), kind=kOutput, calls=%fused_computation.197 | convolution fusion | flops 2097152 | bytes 2103296 | tf_op jit(solution)/shard_map/dot_general | solution.py:25
  28.5 7.6 %all-gather.1 = f32[4,2,4]{2,1,0:T(2,128)S(1)} all-gather(f32[1,2,4]{2,1,0:T(2,128)S(1)} %bitcast.153), channel_id=2, replica_groups=mesh['grp'=2,'sp'=4,'tp'=4] {'sp'}, dimensions={0}, use_global_device_ids=true | all-gather | bytes 160 | tf_op jit(solution)/shard_map/all_gather | solution.py:132
  36.2 10.5 %all-reduce = (bf16[3,512]{1,0:T(4,128)(2,1)S(1)}, bf16[3,256]{1,0:T(4,128)(2,1)S(1)}, bf16[3,256]{1,0:T(4,128)(2,1)S(1)}) all-reduce(bf16[3,512]{1,0:T(4,128)(2,1)S(1)} %get-tuple-element.53, bf16[3,256]{1,0:T(4,128)(2,1)S(1)} %get-tuple-element.56, ...), channel_id=1, replica_groups=mesh['grp'=2,'sp'=4,'tp'=4] {'sp'}, use_global_device_ids=true, to_apply=%region_7.8 | all-reduce | flops 3072 | bytes 12288 | tf_op jit(solution)/shard_map/psum | solution.py:21
  46.7 0.7 convert_convert_fusion
  47.5 1.0 copy.149
  48.6 0.7 convert_reduce_fusion.1
  49.4 2.4 %fusion.90 = (f32[4,128,2,4]{3,2,1,0:T(2,128)}, f32[4,128,2,4]{3,2,1,0:T(2,128)S(1)}) fusion(f32[4,128,2,4]{3,2,1,0:T(2,128)S(1)} %fusion.94, f32[4,128,2,4]{3,2,1,0:T(2,128)} %copy.149, f32[4,2,4]{2,1,0:T(2,128)S(1)} %get-tuple-element.47), kind=kLoop, calls=%fused_computation.187 | loop fusion | flops 8192 | bytes 65664 | tf_op jit(solution)/shard_map/exp | solution.py:164
  51.8 0.7 convert_reduce_fusion
  53.2 0.6 mul.552
  53.9 0.7 mul.510
  54.6 0.7 mul.529
  55.7 1.2 copy.148
  57.7 1.0 maximum_convert_fusion.2
  58.7 1.0 multiply_convert_fusion.5
  59.8 0.7 maximum_convert_fusion.1
  60.6 1.2 maximum_convert_fusion
  61.8 1.3 %multiply_convert_fusion.4 = bf16[512,512]{1,0:T(8,128)(2,1)S(1)} fusion(f32[515,512]{1,0:T(8,128)S(1)} %maximum_convert_fusion, f32[512]{0:T(512)} %bitcast.142, f32[512]{0:T(512)} %bitcast.141, f32[512]{0:T(512)} %bitcast.140, f32[512]{0:T(512)} %bitcast.139), kind=kLoop, calls=%fused_computation.44 | loop fusion | flops 3145728 | bytes 4726784 | tf_op jit(solution)/shard_map/convert_element_type | solution.py:103
  63.1 1.0 copy.140
  64.1 2.0 %reshape.229 = bf16[4,128,2,4,64]{1,0,4,3,2:T(4,128)(2,1)} reshape(bf16[512,512]{0,1:T(8,128)(2,1)} %copy.140) | data formatting | bytes 1048576 | tf_op jit(solution)/shard_map/reshape | solution.py:109
  66.1 1.3 %multiply_convert_fusion.3 = bf16[4,128,2,4,64]{1,0,4,3,2:T(4,128)(2,1)S(1)} fusion(bf16[4,128,2,4,64]{1,0,4,3,2:T(4,128)(2,1)} %reshape.229, f32[4,128,2,4]{1,0,3,2:T(4,128)S(1)} %copy.150), kind=kLoop, calls=%fused_computation.38 | loop fusion | flops 786432 | bytes 1064960 | tf_op jit(solution)/shard_map/convert_element_type | solution.py:118
  67.8 1.1 slice_add_fusion
  68.8 1.2 copy.153
  70.0 1.2 reshape.274
  71.2 4.2 %all-to-all-start = ((f32[4,1,16384]{2,1,0:T(1,128)}), f32[4,1,16384]{2,1,0:T(1,128)}, u32[]{:S(2)}, u32[]{:S(2)}) async-start(f32[4,1,16384]{2,1,0:T(1,128)} %reshape.274), calls=%async_computation | async-start | bytes 524288 | tf_op jit(solution)/shard_map/all_to_all | solution.py:136
  75.5 1.0 multiply_convert_fusion.6
  76.5 1.0 reshape.230
  77.6 1.1 fusion.40
  78.7 3.5 %all-to-all-done = f32[4,1,16384]{2,1,0:T(1,128)} async-done(((f32[4,1,16384]{2,1,0:T(1,128)}), f32[4,1,16384]{2,1,0:T(1,128)}, u32[]{:S(2)}, u32[]{:S(2)}) %all-to-all-start) | async-done | bytes 262176 | tf_op jit(solution)/shard_map/all_to_all | solution.py:136
  82.7 2.3 %reduce.9 = f32[4,16384]{1,0:T(4,128)S(1)} reduce(f32[4,1,16384]{2,1,0:T(1,128)} %all-to-all-done, f32[]{:T(128)} %broadcast.118), dimensions={1}, to_apply=%all_to_all.6.reduce_sub_computation | reduce | bytes 524292 | tf_op jit(solution)/shard_map/all_to_all | solution.py:136
  85.3 1.3 %fusion.35 = bf16[2,4,1,32,64]{4,2,3,1,0:T(2,128)(2,1)S(1)} fusion(f32[4,2,4,1,1]{0,3,4,2,1:T(1,128)S(1)} %copy.173, f32[4,32,2,4,64]{4,3,2,1,0:T(4,128)S(1)} %bitcast.123), kind=kOutput, calls=%fused_computation.69 | convolution fusion | flops 786432 | bytes 295040 | tf_op jit(solution)/shard_map/kge,kngep->ngep/dot_general | solution.py:144
  87.0 1.5 %collective-permute-start.3 = (f32[2,4,64]{2,1,0:T(4,128)S(1)}, f32[2,4,64]{2,1,0:T(4,128)S(1)}, u32[]{:S(2)}, u32[]{:S(2)}) collective-permute-start(f32[2,4,64]{2,1,0:T(4,128)S(1)} %bitcast.137), channel_id=1, source_target_pairs={{0,4},{4,0},{8,12},{12,8},{1,5},{5,1},{9,13},{13,9},{2,6},{6,2},{1... | collective-permute-start | bytes 6152 | tf_op jit(solution)/shard_map/ppermute | solution.py:202
  88.5 3.1 %convolution_bitcast_fusion.2 = f32[4,128,2,4,64]{1,4,3,2,0:T(8,128)} fusion(f32[4,2,4,128]{3,2,1,0:T(4,128)S(1)} %copy.146, f32[4,2,4,128]{3,2,1,0:T(4,128)S(1)} %copy.144, f32[4,2,128,128]{3,2,1,0:T(8,128)} %fusion.40, pred[128,128]{1,0:T(8,128)(4,1)S(1)} %iota_compare_fusion, bf16[4,128,2,4,64]{1,0,4,3,2:T(4,128)(2,1)} %reshape.229), kind=kOutput, calls=%fused_computation.5 | convolution fusion | flops 69730304 | bytes 2146304 | tf_op jit(solution)/shard_map/bgels,bsgep->blgep/dot_general | solution.py:160
  91.7 1.3 %collective-permute-start.4 = (f32[2,4,64]{2,1,0:T(4,128)S(1)}, f32[2,4,64]{2,1,0:T(4,128)S(1)}, u32[]{:S(2)}, u32[]{:S(2)}) collective-permute-start(f32[2,4,64]{2,1,0:T(4,128)S(1)} %add.240), channel_id=1, source_target_pairs={{0,8},{4,12},{8,0},{12,4},{1,9},{5,13},{9,1},{13,5},{2,10},{6,14},... | collective-permute-start | bytes 6152 | tf_op jit(solution)/shard_map/ppermute | solution.py:202
  93.0 1.3 %convolution_bitcast_fusion.3 = f32[4,32,2,4,64]{4,0,1,3,2:T(4,128)S(1)} fusion(f32[4,32,2,4,64]{4,3,2,1,0:T(4,128)S(1)} %bitcast.124, f32[4,2,4]{0,2,1:T(4,128)S(1)} %copy.156, f32[4,2,4]{0,2,1:T(4,128)S(1)} %copy.155, pred[4,4]{1,0:T(4,128)(4,1)S(1)} %copy-done.28), kind=kOutput, calls=%fused_computation.10 | convolution fusion | flops 3145984 | bytes 524560 | tf_op jit(solution)/shard_map/jkge,kngep->jngep/dot_general | solution.py:140
  94.5 1.0 reshape.276
  95.5 3.8 %all-to-all-start.1 = ((f32[4,1,16384]{2,1,0:T(1,128)}), f32[4,1,16384]{2,1,0:T(1,128)S(1)}, u32[]{:S(2)}, u32[]{:S(2)}) async-start(f32[4,1,16384]{2,1,0:T(1,128)} %reshape.276), calls=%async_computation.1 | async-start | bytes 524288 | tf_op jit(solution)/shard_map/all_to_all | solution.py:147
  99.3 0.7 convert_element_type.211
  100.4 0.8 multiply_convert_fusion.7
  101.4 0.6 copy.168
  102.0 3.8 %all-to-all-done.1 = f32[4,1,16384]{2,1,0:T(1,128)S(1)} async-done(((f32[4,1,16384]{2,1,0:T(1,128)}), f32[4,1,16384]{2,1,0:T(1,128)S(1)}, u32[]{:S(2)}, u32[]{:S(2)}) %all-to-all-start.1) | async-done | bytes 262176 | tf_op jit(solution)/shard_map/all_to_all | solution.py:147
  105.8 1.3 %reduce.10 = f32[4,16384]{1,0:T(4,128)S(1)} reduce(f32[4,1,16384]{2,1,0:T(1,128)S(1)} %all-to-all-done.1, f32[]{:T(128)} %broadcast.118), dimensions={1}, to_apply=%all_to_all.8.reduce_sub_computation | reduce | bytes 524292 | tf_op jit(solution)/shard_map/all_to_all | solution.py:147
  107.5 0.9 copy.160
  108.4 2.3 %fusion.1 = f32[4,128,2,4,64]{1,4,3,2,0:T(8,128)S(1)} fusion(f32[4,128,2,4,64]{1,4,3,2,0:T(8,128)} %convolution_bitcast_fusion.2, f32[1,128,2,4,64]{1,4,3,2,0:T(8,128)} %get-tuple-element.41, f32[1,128,2,4,64]{1,4,3,2,0:T(8,128)} %get-tuple-element.42, f32[1,128,2,4,64]{1,4,3,2,0:T(8,128)} %get-tuple-element.43, f32[4]{0:T(128)S(1)} %copy-done.29, ...), kind=kOutput, calls=%fused_computation.4 | convolution fusion | flops 404488192 | bytes 3424400 | tf_op jit(solution)/shard_map/blgn,bngep->blgep/dot_general | solution.py:164
  110.7 1.8 %copy.184 = f32[4,128,2,4,64]{4,3,2,1,0:T(4,128)} copy(f32[4,128,2,4,64]{1,4,3,2,0:T(8,128)S(1)} %fusion.1) | data formatting | bytes 2097152 | tf_op jit(solution)/shard_map/reshape | solution.py:170
  112.5 3.5 %reshape.263 = f32[512,512]{1,0:T(8,128)} reshape(f32[4,128,2,4,64]{4,3,2,1,0:T(4,128)} %copy.184) | data formatting | bytes 2097152 | tf_op jit(solution)/shard_map/reshape | solution.py:170
  116.0 4.6 %fusion.93 = (f32[512,512]{1,0:T(8,128)}, f32[512,512]{1,0:T(8,128)}) fusion(bf16[512,2048]{1,0:T(8,128)(2,1)S(1)} %copy-done, bf16[2048,512]{1,0:T(8,128)(2,1)} %param.20, f32[512,512]{1,0:T(8,128)} %reshape.263, bf16[512,512]{1,0:T(8,128)(2,1)S(1)} %copy-done.2, f32[512]{0:T(512)S(1)} %copy-done.23), kind=kOutput, calls=%fused_computation.190 | convolution fusion | flops 1076625408 | bytes 7866368 | tf_op jit(solution)/shard_map/dot_general | solution.py:25
  120.6 1.9 %mul.516 = f32[512,2,256]{2,1,0:T(2,128)S(1)} reshape(f32[512,512]{1,0:T(8,128)} %get-tuple-element.63) | data formatting | bytes 2097152 | tf_op jit(solution)/shard_map/mul | solution.py:39
  122.5 0.6 reduce_sum.28
  123.2 0.6 mul.517
  124.3 1.1 multiply_convert_fusion.2
  (130 shorter events, 7.8 us)
Async XLA Ops:
  0.6 1.6 %copy-start = (bf16[512,2048]{1,0:T(8,128)(2,1)S(1)}, bf16[512,2048]{1,0:T(8,128)(2,1)}, u32[]{:S(2)}) copy-start(bf16[512,2048]{1,0:T(8,128)(2,1)} %param.15) | copy-start | bytes 6291460
  0.6 9.8 %copy-start.6 = (bf16[2048,256]{1,0:T(8,128)(2,1)S(1)}, bf16[2048,256]{1,0:T(8,128)(2,1)}, u32[]{:S(2)}) copy-start(bf16[2048,256]{1,0:T(8,128)(2,1)} %param.19) | copy-start | bytes 3145732
  4.2 7.6 %copy-start.9 = (bf16[512,256]{1,0:T(8,128)(2,1)}, bf16[512,256]{1,0:T(8,128)(2,1)S(1)}, u32[]{:S(2)}) copy-start(bf16[512,256]{1,0:T(8,128)(2,1)S(1)} %convolution_convert_fusion.2) | copy-start | bytes 786436
  4.2 11.2 %copy-start.3 = (bf16[2048,512]{1,0:T(8,128)(2,1)S(1)}, bf16[2048,512]{1,0:T(8,128)(2,1)}, u32[]{:S(2)}) copy-start(bf16[2048,512]{1,0:T(8,128)(2,1)} %param.17) | copy-start | bytes 6291460
  4.8 52.9 %collective-permute-start.2 = (bf16[3,256]{1,0:T(4,128)(2,1)}, bf16[3,256]{1,0:T(4,128)(2,1)}, u32[]{:S(2)}, u32[]{:S(2)}) collective-permute-start(bf16[3,256]{1,0:T(4,128)(2,1)} %get-tuple-element.57), channel_id=1, source_target_pairs={{0,4},{4,8},{8,12},{1,5},{5,9},{9,13},{2,6},{6,10},{10,14},{3,7},{... | collective-permute-start | bytes 4616 | tf_op jit(solution)/shard_map/ppermute | solution.py:16
  11.8 10.3 %copy-start.21 = (bf16[2048]{0:T(1024)(128)(2,1)S(1)}, bf16[2048]{0:T(1024)(128)(2,1)}, u32[]{:S(2)}) copy-start(bf16[2048]{0:T(1024)(128)(2,1)} %param.16) | copy-start | bytes 12292
  11.8 10.3 %copy-start.5 = (bf16[2048,256]{1,0:T(8,128)(2,1)S(1)}, bf16[2048,256]{1,0:T(8,128)(2,1)}, u32[]{:S(2)}) copy-start(bf16[2048,256]{1,0:T(8,128)(2,1)} %param.18) | copy-start | bytes 3145732
  11.8 48.0 %collective-permute-start.1 = (bf16[3,256]{1,0:T(4,128)(2,1)}, bf16[3,256]{1,0:T(4,128)(2,1)}, u32[]{:S(2)}, u32[]{:S(2)}) collective-permute-start(bf16[3,256]{1,0:T(4,128)(2,1)} %get-tuple-element.54), channel_id=1, source_target_pairs={{0,4},{4,8},{8,12},{1,5},{5,9},{9,13},{2,6},{6,10},{10,14},{3,7},{... | collective-permute-start | bytes 4616 | tf_op jit(solution)/shard_map/ppermute | solution.py:16
  16.7 0.8 copy-start.8
  18.1 42.5 %collective-permute-start = (bf16[3,512]{1,0:T(4,128)(2,1)}, bf16[3,512]{1,0:T(4,128)(2,1)}, u32[]{:S(2)}, u32[]{:S(2)}) collective-permute-start(bf16[3,512]{1,0:T(4,128)(2,1)} %get-tuple-element.52), channel_id=1, source_target_pairs={{0,4},{4,8},{8,12},{1,5},{5,9},{9,13},{2,6},{6,10},{10,14},{3,7},{... | collective-permute-start | bytes 9224 | tf_op jit(solution)/shard_map/ppermute | solution.py:16
  21.6 2.3 %copy-start.4 = (bf16[2048,512]{1,0:T(8,128)(2,1)S(1)}, bf16[2048,512]{1,0:T(8,128)(2,1)}, u32[]{:S(2)}) copy-start(bf16[2048,512]{1,0:T(8,128)(2,1)} %param.17) | copy-start | bytes 6291460
  22.1 2.2 %copy-start.31 = (f32[32]{0:T(128)S(1)}, f32[32]{0:T(128)}, u32[]{:S(2)}) copy-start(f32[32]{0:T(128)} %param.26) | copy-start | bytes 388
  22.1 2.3 %copy-start.30 = (f32[32]{0:T(128)S(1)}, f32[32]{0:T(128)}, u32[]{:S(2)}) copy-start(f32[32]{0:T(128)} %param.25) | copy-start | bytes 388
  22.1 2.4 %copy-start.10 = (f32[512,8]{0,1:T(8,128)S(1)}, f32[512,8]{0,1:T(8,128)}, u32[]{:S(2)}) copy-start(f32[512,8]{0,1:T(8,128)} %param.27) | copy-start | bytes 49156
  22.4 2.0 %copy-start.11 = (bf16[2048,32]{0,1:T(8,128)(2,1)S(1)}, bf16[2048,32]{0,1:T(8,128)(2,1)}, u32[]{:S(2)}) copy-start(bf16[2048,32]{0,1:T(8,128)(2,1)} %param.21) | copy-start | bytes 393220
  25.2 21.5 %copy-start.24 = (bf16[4,1024]{1,0:T(4,128)(2,1)S(1)}, bf16[4,1024]{1,0:T(4,128)(2,1)}, u32[]{:S(2)}) copy-start(bf16[4,1024]{1,0:T(4,128)(2,1)} %param.23) | copy-start | bytes 24580
  25.5 23.0 %copy-start.25 = (bf16[4,1024]{1,0:T(4,128)(2,1)S(1)}, bf16[4,1024]{1,0:T(4,128)(2,1)}, u32[]{:S(2)}) copy-start(bf16[4,1024]{1,0:T(4,128)(2,1)} %param.24) | copy-start | bytes 24580
  26.5 25.3 %copy-start.20 = (bf16[4,2048]{1,0:T(4,128)(2,1)S(1)}, bf16[4,2048]{1,0:T(4,128)(2,1)}, u32[]{:S(2)}) copy-start(bf16[4,2048]{1,0:T(4,128)(2,1)} %param.22) | copy-start | bytes 49156
  26.5 26.6 %copy-start.32 = (f32[32]{0:T(128)S(1)}, f32[32]{0:T(128)}, u32[]{:S(2)}) copy-start(f32[32]{0:T(128)} %param.28) | copy-start | bytes 388
  63.1 4.6 %copy-start.1 = (bf16[512,512]{1,0:T(8,128)(2,1)}, bf16[512,512]{1,0:T(8,128)(2,1)S(1)}, u32[]{:S(2)}) copy-start(bf16[512,512]{1,0:T(8,128)(2,1)S(1)} %multiply_convert_fusion.4) | copy-start | bytes 1572868
  66.1 1.6 %copy-start.12 = (f32[2,4]{1,0:T(2,128)S(1)}, f32[2,4]{1,0:T(2,128)}, u32[]{:S(2)}) copy-start(f32[2,4]{1,0:T(2,128)} %get-tuple-element.48) | copy-start | bytes 100
  66.1 1.6 %copy-start.13 = (f32[2,4]{1,0:T(2,128)S(1)}, f32[2,4]{1,0:T(2,128)}, u32[]{:S(2)}) copy-start(f32[2,4]{1,0:T(2,128)} %get-tuple-element.49) | copy-start | bytes 100
  66.1 1.6 %copy-start.14 = (f32[2,4]{1,0:T(2,128)S(1)}, f32[2,4]{1,0:T(2,128)}, u32[]{:S(2)}) copy-start(f32[2,4]{1,0:T(2,128)} %get-tuple-element.50) | copy-start | bytes 100
  66.1 1.6 %copy-start.15 = (f32[2,4]{1,0:T(2,128)S(1)}, f32[2,4]{1,0:T(2,128)}, u32[]{:S(2)}) copy-start(f32[2,4]{1,0:T(2,128)} %get-tuple-element.51) | copy-start | bytes 100
  67.7 7.7 %copy-start.16 = (f32[1,256]{1,0:T(1,128)S(1)}, f32[1,256]{1,0:T(1,128)}, u32[]{:S(2)}) copy-start(f32[1,256]{1,0:T(1,128)} %get-tuple-element.24) | copy-start | bytes 3076
  67.7 7.7 %copy-start.17 = (f32[1,256]{1,0:T(1,128)S(1)}, f32[1,256]{1,0:T(1,128)}, u32[]{:S(2)}) copy-start(f32[1,256]{1,0:T(1,128)} %get-tuple-element.25) | copy-start | bytes 3076
  67.7 7.7 %copy-start.18 = (f32[1,256]{1,0:T(1,128)S(1)}, f32[1,256]{1,0:T(1,128)}, u32[]{:S(2)}) copy-start(f32[1,256]{1,0:T(1,128)} %get-tuple-element.26) | copy-start | bytes 3076
  67.7 7.7 %copy-start.19 = (f32[1,256]{1,0:T(1,128)S(1)}, f32[1,256]{1,0:T(1,128)}, u32[]{:S(2)}) copy-start(f32[1,256]{1,0:T(1,128)} %get-tuple-element.27) | copy-start | bytes 3076
  71.2 10.9 %all-to-all-start = ((f32[4,1,16384]{2,1,0:T(1,128)}), f32[4,1,16384]{2,1,0:T(1,128)}, u32[]{:S(2)}, u32[]{:S(2)}) async-start(f32[4,1,16384]{2,1,0:T(1,128)} %reshape.274), calls=%async_computation | async-start | bytes 524288 | tf_op jit(solution)/shard_map/all_to_all | solution.py:136
  76.5 10.1 %copy-start.26 = (f32[2,4]{1,0:T(2,128)S(1)}, f32[2,4]{1,0:T(2,128)}, u32[]{:S(2)}) copy-start(f32[2,4]{1,0:T(2,128)} %mul.529) | copy-start | bytes 100
  76.5 10.3 %copy-start.22 = (bf16[2,32,1,1]{1,0,2,3:T(2,128)(2,1)S(1)}, bf16[2,32,1,1]{1,0,2,3:T(2,128)(2,1)}, u32[]{:S(2)}) copy-start(bf16[2,32,1,1]{1,0,2,3:T(2,128)(2,1)} %fusion.81) | copy-start | bytes 388
  86.8 6.2 %copy-start.28 = (pred[4,4]{1,0:T(4,128)(4,1)S(1)}, pred[4,4]{1,0:T(4,128)(4,1)}, u32[]{:S(2)}) copy-start(pred[4,4]{1,0:T(4,128)(4,1)} %iota_compare_fusion.1) | copy-start | bytes 52
  87.0 4.7 %collective-permute-start.3 = (f32[2,4,64]{2,1,0:T(4,128)S(1)}, f32[2,4,64]{2,1,0:T(4,128)S(1)}, u32[]{:S(2)}, u32[]{:S(2)}) collective-permute-start(f32[2,4,64]{2,1,0:T(4,128)S(1)} %bitcast.137), channel_id=1, source_target_pairs={{0,4},{4,0},{8,12},{12,8},{1,5},{5,1},{9,13},{13,9},{2,6},{6,2},{1... | collective-permute-start | bytes 6152 | tf_op jit(solution)/shard_map/ppermute | solution.py:202
  91.7 8.4 %copy-start.27 = (f32[2,4]{1,0:T(2,128)S(1)}, f32[2,4]{1,0:T(2,128)}, u32[]{:S(2)}) copy-start(f32[2,4]{1,0:T(2,128)} %mul.552) | copy-start | bytes 100
  91.7 8.4 %collective-permute-start.4 = (f32[2,4,64]{2,1,0:T(4,128)S(1)}, f32[2,4,64]{2,1,0:T(4,128)S(1)}, u32[]{:S(2)}, u32[]{:S(2)}) collective-permute-start(f32[2,4,64]{2,1,0:T(4,128)S(1)} %add.240), channel_id=1, source_target_pairs={{0,8},{4,12},{8,0},{12,4},{1,9},{5,13},{9,1},{13,5},{2,10},{6,14},... | collective-permute-start | bytes 6152 | tf_op jit(solution)/shard_map/ppermute | solution.py:202
  95.5 12.9 %copy-start.29 = (f32[4]{0:T(128)S(1)}, f32[4]{0:T(128)}, u32[]{:S(2)}) copy-start(f32[4]{0:T(128)} %pad.6.clone) | copy-start | bytes 52
  95.5 10.3 %all-to-all-start.1 = ((f32[4,1,16384]{2,1,0:T(1,128)}), f32[4,1,16384]{2,1,0:T(1,128)S(1)}, u32[]{:S(2)}, u32[]{:S(2)}) async-start(f32[4,1,16384]{2,1,0:T(1,128)} %reshape.276), calls=%async_computation.1 | async-start | bytes 524288 | tf_op jit(solution)/shard_map/all_to_all | solution.py:147
  112.5 3.5 %copy-start.2 = (bf16[512,512]{1,0:T(8,128)(2,1)S(1)}, bf16[512,512]{1,0:T(8,128)(2,1)}, u32[]{:S(2)}) copy-start(bf16[512,512]{1,0:T(8,128)(2,1)} %copy-done.1) | copy-start | bytes 1572868
  112.5 3.5 %copy-start.23 = (f32[512]{0:T(512)S(1)}, f32[512]{0:T(512)}, u32[]{:S(2)}) copy-start(f32[512]{0:T(512)} %mul.510) | copy-start | bytes 6148
  123.1 1.2 copy-start.7
